TPU v7x, 128 devices: a whole 4x4x4 slice. The times are simulated.
128 devices in a mesh: ep: 128 (over z, y, x, core).
Axes of the slice: x: 4, y: 4, z: 4, core: 2. Of those that a mesh axis runs over, the one named last changes fastest.
Arguments:
- tokens: bfloat16 [4096, 3072], P('ep'), may hold values from -6 to 6
- norm_gain: float32 [3072], replicated, may hold values from 0.1 to 1.9
- expert_ids: int32 [4096, 4], P('ep'), may hold values from 0 to 127, as said below
- expert_scores: float32 [4096, 4], P('ep'), may hold values from -100 to 180
- group_prob: float32 [4096], P('ep'), may hold values from 0.25 to 1
- gate_weight: bfloat16 [128, 3072, 384], P('ep'), may hold values from -0.109375 to 0.109375
- up_weight: bfloat16 [128, 3072, 384], P('ep'), may hold values from -0.109375 to 0.109375
- down_weight: bfloat16 [128, 384, 3072], P('ep'), may hold values from -0.3125 to 0.3125
Outputs:
- combined: bfloat16 [4096, 3072], P('ep')
Inputs may be any that keep to these rules, and one draw needn't show every extreme that they name: `expert_ids`: the 4 ids of a row are different and lie in one group of 32 consecutive experts. Among the rows of one device no expert is named by more than 4 rows, and in every draw some expert is named by exactly 4 rows of one device.
All inputs are finite; a program needn't handle non-finite values.
Results may differ from a plain program's by a relative error of at most 0.0085.
Values may be sent and summed in bfloat16 or wider, within the bound.
A program may use at most 128 MiB of HBM per device.

v0:
```python
import jax
import jax.numpy as jnp
from jax import lax
from jax.sharding import PartitionSpec as P

GROUPS = 4
TOP_K = 4


eps_norm = 1e-05


def items_in_groups(value, axis, split_dim, concat_dim, work, item_dim, out_dim):

    def moved(group):
        return lax.all_to_all(group, axis, split_axis=split_dim, concat_axis=concat_dim, tiled=True)

    items = jax.tree.leaves(value)[0].shape[item_dim]
    ends = [items * k // 2 for k in range(2 + 1)] if items % 2 == 0 else [0, items]
    groups = [
        jax.tree.map(lambda a: lax.slice_in_dim(a, low, high, axis=item_dim), value)
        for low, high in zip(ends, ends[1:])
    ]
    arrived = [moved(group) for group in groups]
    made = [work(group) for group in arrived]
    return jax.tree.map(lambda *parts: jnp.concatenate(parts, axis=out_dim), *made)


def layer_norm(tokens, norm_gain):
    values = tokens.astype(jnp.float32)
    average = jnp.mean(values, axis=1, keepdims=True)
    centred = values - average
    variance = jnp.mean(centred * centred, axis=1, keepdims=True)
    return (centred * lax.rsqrt(variance + eps_norm) * norm_gain[None, :]).astype(jnp.bfloat16)


def mixing_weights(expert_scores, group_prob):
    shifted = expert_scores - jnp.max(expert_scores, axis=1, keepdims=True)
    exp_scores = jnp.exp(shifted)
    return exp_scores / jnp.sum(exp_scores, axis=1, keepdims=True) * group_prob[:, None]


def expert_rows(flat_rows, gate_matrix, up_matrix, down_matrix):
    gate_act = jnp.dot(flat_rows, gate_matrix, preferred_element_type=jnp.float32)
    up_act = jnp.dot(flat_rows, up_matrix, preferred_element_type=jnp.float32)
    hidden = (jax.nn.silu(gate_act) * up_act).astype(jnp.bfloat16)
    return jnp.dot(hidden, down_matrix, preferred_element_type=jnp.float32).astype(jnp.bfloat16)


def local(
    tokens, norm_gain, expert_ids, expert_scores, group_prob, gate_weight, up_weight, down_weight
):
    normed = layer_norm(tokens, norm_gain)
    weights_tok = mixing_weights(expert_scores, group_prob)
    tok_count = tokens.shape[0]
    model_width = tokens.shape[1]
    expert_count = lax.axis_size("ep")
    group_size = expert_count // GROUPS
    capacity = (tok_count * TOP_K + group_size - 1) // group_size
    expert_iota = jnp.arange(expert_count, dtype=jnp.int32)
    slot_iota = jnp.arange(capacity, dtype=jnp.int32)
    matches = expert_ids[:, :, None] == expert_iota[None, None, :]
    route_weight = jnp.sum(jnp.where(matches, weights_tok[:, :, None], 0.0), axis=1)
    gate_matrix = gate_weight[0]
    up_matrix = up_weight[0]
    down_matrix = down_weight[0]
    chosen = jnp.sum(matches.astype(jnp.int32), axis=1)
    order_rank = jnp.cumsum(chosen, axis=0) - chosen
    slot_map = (chosen.T[:, None, :] == 1) & (order_rank.T[:, None, :] == slot_iota[None, :, None])
    outgoing = jnp.einsum(
        "emt,td->emd", slot_map.astype(jnp.bfloat16), normed, preferred_element_type=jnp.float32
    ).astype(jnp.bfloat16)

    def serve_rows(received):
        flat_rows = received.reshape(-1, model_width)
        results = expert_rows(flat_rows, gate_matrix, up_matrix, down_matrix).reshape(
            received.shape
        )
        return lax.all_to_all(results, "ep", split_axis=0, concat_axis=0, tiled=True)

    returned_rows = items_in_groups(outgoing, "ep", 0, 0, serve_rows, 1, 1)
    slot_scale = jnp.where(slot_map, route_weight.T[:, None, :], 0.0)
    mixture = jnp.einsum("emt,emd->td", slot_scale, returned_rows.astype(jnp.float32))
    return mixture.astype(jnp.bfloat16)


def solution(mesh):
    in_specs = (
        P("ep", None),
        P(),
        P("ep", None),
        P("ep", None),
        P("ep"),
        P("ep", None, None),
        P("ep", None, None),
        P("ep", None, None),
    )
    out_specs = P("ep", None)
    return jax.shard_map(local, mesh=mesh, in_specs=in_specs, out_specs=out_specs, check_vma=False)
```

profile of v0, /device:TPU:1, one launch (start us, length us, event | category | flops | bytes accessed | tf_op | source)
XLA Modules:
  0.0 139.5 jit_solution(2050878773544634225)
XLA Ops:
  0.0 0.0 copy-start
  0.0 0.9 convert_reduce_fusion.1
  0.9 0.1 reduce_window_sum.11
  1.0 1.1 convert_reduce_fusion
  2.1 1.2 fusion.32
  3.2 2.0 %convolution_convert_fusion = bf16[128,4,3072]{2,0,1:T(8,128)(2,1)S(1)} fusion(bf16[32,3072]{1,0:T(8,128)(2,1)} %param.8, f32[3072]{0:T(1024)} %param.9, f32[32]{0:T(128)S(1)} %add_rsqrt_fusion, f32[32]{0:T(128)S(1)} %broadcast_multiply_fusion, s32[128,32]{0,1:T(8,128)S(1)} %subtract_bitcast_fusion, pred[128,32]{0,1:T(8,128)(4,1)S(1)} %compare_bitcast_fusion), kind=kOutput, calls=%fused_computation | convolution fusion | flops 102760448 | bytes 3375360 | tf_op jit(solution)/shard_map/emt,td->emd/dot_general | solution.py:70
  5.2 1.4 fusion.67
  6.6 2.8 %copy.25 = bf16[128,2,3072]{2,1,0:T(2,128)(2,1)} copy(bf16[128,2,3072]{2,0,1:T(8,128)(2,1)S(1)} %get-tuple-element.5) | data formatting | bytes 3145728 | tf_op jit(solution)/shard_map/slice | solution.py:21
  9.4 11.9 %all-to-all-start = ((bf16[128,2,3072]{2,1,0:T(2,128)(2,1)}), bf16[128,2,3072]{2,1,0:T(2,128)(2,1)}, u32[]{:S(2)}, u32[]{:S(2)}) async-start(bf16[128,2,3072]{2,1,0:T(2,128)(2,1)} %copy.25), calls=%async_computation | async-start | bytes 3145728 | tf_op jit(solution)/shard_map/all_to_all | solution.py:16
  21.3 4.2 %copy.26 = bf16[128,2,3072]{2,1,0:T(2,128)(2,1)} copy(bf16[128,2,3072]{2,0,1:T(8,128)(2,1)} %get-tuple-element.6) | data formatting | bytes 3145728 | tf_op jit(solution)/shard_map/slice | solution.py:21
  25.4 20.4 %all-to-all-done = bf16[128,2,3072]{2,1,0:T(2,128)(2,1)} async-done(((bf16[128,2,3072]{2,1,0:T(2,128)(2,1)}), bf16[128,2,3072]{2,1,0:T(2,128)(2,1)}, u32[]{:S(2)}, u32[]{:S(2)}) %all-to-all-start) | async-done | bytes 1572896 | tf_op jit(solution)/shard_map/all_to_all | solution.py:16
  45.8 5.4 %all-to-all-start.2 = ((bf16[128,2,3072]{2,1,0:T(2,128)(2,1)}), bf16[128,2,3072]{2,1,0:T(2,128)(2,1)}, u32[]{:S(2)}, u32[]{:S(2)}) async-start(bf16[128,2,3072]{2,1,0:T(2,128)(2,1)} %copy.26), calls=%async_computation.2 | async-start | bytes 3145728 | tf_op jit(solution)/shard_map/all_to_all | solution.py:16
  51.2 4.6 %reshape.34 = bf16[256,3072]{1,0:T(8,128)(2,1)} reshape(bf16[128,2,3072]{2,1,0:T(2,128)(2,1)} %all-to-all-done) | data formatting | bytes 3145728 | tf_op jit(solution)/shard_map/reshape | solution.py:75
  55.9 3.1 %fusion.12 = f32[256,384]{1,0:T(8,128)S(1)} fusion(bf16[256,3072]{1,0:T(8,128)(2,1)} %reshape.34, bf16[1,3072,384]{2,1,0:T(8,128)(2,1)} %param.13), kind=kOutput, calls=%fused_computation.16 | convolution fusion | flops 603979776 | bytes 4325376 | tf_op jit(solution)/shard_map/dot_general | solution.py:44
  59.0 0.0 copy-done
  59.0 5.2 %convolution_convert_fusion.2 = bf16[256,3072]{1,0:T(8,128)(2,1)} fusion(bf16[1,384,3072]{2,1,0:T(8,128)(2,1)S(1)} %copy-done, bf16[256,3072]{1,0:T(8,128)(2,1)} %reshape.34, bf16[1,3072,384]{2,1,0:T(8,128)(2,1)} %param.14, f32[256,384]{1,0:T(8,128)S(1)} %fusion.12), kind=kOutput, calls=%fused_computation.2 | convolution fusion | flops 1209335808 | bytes 8257536 | tf_op jit(solution)/shard_map/dot_general | solution.py:47
  64.2 4.5 %reshape.35 = bf16[128,2,3072]{2,1,0:T(2,128)(2,1)} reshape(bf16[256,3072]{1,0:T(8,128)(2,1)} %convolution_convert_fusion.2) | data formatting | bytes 3145728 | tf_op jit(solution)/shard_map/reshape | solution.py:76
  68.7 7.2 %all-to-all-done.2 = bf16[128,2,3072]{2,1,0:T(2,128)(2,1)} async-done(((bf16[128,2,3072]{2,1,0:T(2,128)(2,1)}), bf16[128,2,3072]{2,1,0:T(2,128)(2,1)}, u32[]{:S(2)}, u32[]{:S(2)}) %all-to-all-start.2) | async-done | bytes 1572896 | tf_op jit(solution)/shard_map/all_to_all | solution.py:16
  75.9 5.6 %all-to-all-start.1 = ((bf16[128,2,3072]{2,1,0:T(2,128)(2,1)}), bf16[128,2,3072]{2,1,0:T(2,128)(2,1)}, u32[]{:S(2)}, u32[]{:S(2)}) async-start(bf16[128,2,3072]{2,1,0:T(2,128)(2,1)} %reshape.35), calls=%async_computation.1 | async-start | bytes 3145728 | tf_op jit(solution)/shard_map/all_to_all | solution.py:79
  81.5 4.6 %reshape.36 = bf16[256,3072]{1,0:T(8,128)(2,1)} reshape(bf16[128,2,3072]{2,1,0:T(2,128)(2,1)} %all-to-all-done.2) | data formatting | bytes 3145728 | tf_op jit(solution)/shard_map/reshape | solution.py:75
  86.1 3.1 %fusion.10 = f32[256,384]{1,0:T(8,128)S(1)} fusion(bf16[256,3072]{1,0:T(8,128)(2,1)} %reshape.36, bf16[1,3072,384]{2,1,0:T(8,128)(2,1)} %param.13), kind=kOutput, calls=%fused_computation.14 | convolution fusion | flops 603979776 | bytes 4325376 | tf_op jit(solution)/shard_map/dot_general | solution.py:44
  89.3 5.2 %convolution_convert_fusion.1 = bf16[256,3072]{1,0:T(8,128)(2,1)} fusion(bf16[1,384,3072]{2,1,0:T(8,128)(2,1)S(1)} %copy-done, bf16[256,3072]{1,0:T(8,128)(2,1)} %reshape.36, bf16[1,3072,384]{2,1,0:T(8,128)(2,1)} %param.14, f32[256,384]{1,0:T(8,128)S(1)} %fusion.10), kind=kOutput, calls=%fused_computation.1 | convolution fusion | flops 1209335808 | bytes 8257536 | tf_op jit(solution)/shard_map/dot_general | solution.py:47
  94.5 4.5 %reshape.37 = bf16[128,2,3072]{2,1,0:T(2,128)(2,1)} reshape(bf16[256,3072]{1,0:T(8,128)(2,1)} %convolution_convert_fusion.1) | data formatting | bytes 3145728 | tf_op jit(solution)/shard_map/reshape | solution.py:76
  98.9 7.2 %all-to-all-done.1 = bf16[128,2,3072]{2,1,0:T(2,128)(2,1)} async-done(((bf16[128,2,3072]{2,1,0:T(2,128)(2,1)}), bf16[128,2,3072]{2,1,0:T(2,128)(2,1)}, u32[]{:S(2)}, u32[]{:S(2)}) %all-to-all-start.1) | async-done | bytes 1572896 | tf_op jit(solution)/shard_map/all_to_all | solution.py:79
  106.2 5.4 %all-to-all-start.3 = ((bf16[128,2,3072]{2,1,0:T(2,128)(2,1)}), bf16[128,2,3072]{2,1,0:T(2,128)(2,1)}, u32[]{:S(2)}, u32[]{:S(2)}) async-start(bf16[128,2,3072]{2,1,0:T(2,128)(2,1)} %reshape.37), calls=%async_computation.3 | async-start | bytes 3145728 | tf_op jit(solution)/shard_map/all_to_all | solution.py:79
  111.6 0.0 copy-done.2
  111.7 0.1 select_reduce_fusion
  111.8 2.9 %copy.27 = bf16[128,2,3072]{2,0,1:T(8,128)(2,1)} copy(bf16[128,2,3072]{2,1,0:T(2,128)(2,1)} %all-to-all-done.1) | data formatting | bytes 3145728 | tf_op jit(solution)/shard_map/all_to_all | solution.py:79
  114.7 21.6 %all-to-all-done.3 = bf16[128,2,3072]{2,1,0:T(2,128)(2,1)} async-done(((bf16[128,2,3072]{2,1,0:T(2,128)(2,1)}), bf16[128,2,3072]{2,1,0:T(2,128)(2,1)}, u32[]{:S(2)}, u32[]{:S(2)}) %all-to-all-start.3) | async-done | bytes 1572896 | tf_op jit(solution)/shard_map/all_to_all | solution.py:79
  136.3 1.9 %copy.28 = bf16[128,2,3072]{2,0,1:T(8,128)(2,1)S(1)} copy(bf16[128,2,3072]{2,1,0:T(2,128)(2,1)} %all-to-all-done.3) | data formatting | bytes 3145728 | tf_op jit(solution)/shard_map/all_to_all | solution.py:79
  138.1 0.0 copy-done.1
  138.1 1.3 fusion
  (13 shorter events, 0.1 us)
Async XLA Ops:
  0.0 59.0 %copy-start = (bf16[1,384,3072]{2,1,0:T(8,128)(2,1)S(1)}, bf16[1,384,3072]{2,1,0:T(8,128)(2,1)}, u32[]{:S(2)}) copy-start(bf16[1,384,3072]{2,1,0:T(8,128)(2,1)} %param.15) | copy-start | bytes 7077892
  9.4 36.4 %all-to-all-start = ((bf16[128,2,3072]{2,1,0:T(2,128)(2,1)}), bf16[128,2,3072]{2,1,0:T(2,128)(2,1)}, u32[]{:S(2)}, u32[]{:S(2)}) async-start(bf16[128,2,3072]{2,1,0:T(2,128)(2,1)} %copy.25), calls=%async_computation | async-start | bytes 3145728 | tf_op jit(solution)/shard_map/all_to_all | solution.py:16
  45.8 30.1 %all-to-all-start.2 = ((bf16[128,2,3072]{2,1,0:T(2,128)(2,1)}), bf16[128,2,3072]{2,1,0:T(2,128)(2,1)}, u32[]{:S(2)}, u32[]{:S(2)}) async-start(bf16[128,2,3072]{2,1,0:T(2,128)(2,1)} %copy.26), calls=%async_computation.2 | async-start | bytes 3145728 | tf_op jit(solution)/shard_map/all_to_all | solution.py:16
  75.9 30.3 %all-to-all-start.1 = ((bf16[128,2,3072]{2,1,0:T(2,128)(2,1)}), bf16[128,2,3072]{2,1,0:T(2,128)(2,1)}, u32[]{:S(2)}, u32[]{:S(2)}) async-start(bf16[128,2,3072]{2,1,0:T(2,128)(2,1)} %reshape.35), calls=%async_computation.1 | async-start | bytes 3145728 | tf_op jit(solution)/shard_map/all_to_all | solution.py:79
  98.9 12.6 %copy-start.2 = (f32[32,4]{0,1:T(4,128)S(1)}, f32[32,4]{0,1:T(4,128)}, u32[]{:S(2)}) copy-start(f32[32,4]{0,1:T(4,128)} %param.11) | copy-start | bytes 1540
  98.9 12.7 %copy-start.4 = (f32[32]{0:T(128)S(1)}, f32[32]{0:T(128)}, u32[]{:S(2)}) copy-start(f32[32]{0:T(128)} %param.12) | copy-start | bytes 388
  98.9 12.7 %copy-start.3 = (s32[32,4]{0,1:T(4,128)S(1)}, s32[32,4]{0,1:T(4,128)}, u32[]{:S(2)}) copy-start(s32[32,4]{0,1:T(4,128)} %param.10) | copy-start | bytes 1540
  106.2 30.1 %all-to-all-start.3 = ((bf16[128,2,3072]{2,1,0:T(2,128)(2,1)}), bf16[128,2,3072]{2,1,0:T(2,128)(2,1)}, u32[]{:S(2)}, u32[]{:S(2)}) async-start(bf16[128,2,3072]{2,1,0:T(2,128)(2,1)} %reshape.37), calls=%async_computation.3 | async-start | bytes 3145728 | tf_op jit(solution)/shard_map/all_to_all | solution.py:79
  136.3 1.9 %copy-start.1 = (bf16[128,2,3072]{2,0,1:T(8,128)(2,1)S(1)}, bf16[128,2,3072]{2,0,1:T(8,128)(2,1)}, u32[]{:S(2)}) copy-start(bf16[128,2,3072]{2,0,1:T(8,128)(2,1)} %copy.27) | copy-start | bytes 4718596
where the time goes:
time: 140 us; the launch traced here: 139 us
  waiting for transfers between devices  56.4 us (40%)
  local copies, waits for them, and re-layouts  31.4 us (22%)
  starting transfers between devices  28.3 us (20%)
  matrix products  20 us (14%)
  other arithmetic  3.36 us (2%)
    all_to_all x2, waiting for transfers between devices, serve_rows(): lax.all_to_all(results, 'ep', split_axis=0, concat_axis=0, tiled=True)  28.8 us
    all_to_all x2, waiting for transfers between devices, moved(): lax.all_to_all(group, axis, split_axis=split_dim, concat_axis=concat_dim,...  27.6 us
    all_to_all x2, starting transfers between devices, moved(): lax.all_to_all(group, axis, split_axis=split_dim, concat_axis=concat_dim,...  17.3 us
    all_to_all x2, starting transfers between devices, serve_rows(): lax.all_to_all(results, 'ep', split_axis=0, concat_axis=0, tiled=True)  11 us
    dot_general x2, matrix products, expert_rows(): jnp.dot(hidden, down_matrix, preferred_element_type=jnp.float32)  10.4 us
    reshape x2, local copies, waits for them, and re-layouts, serve_rows(): flat_rows = received.reshape(-1, model_width)  9.29 us
    reshape x2, local copies, waits for them, and re-layouts, serve_rows(): expert_rows(flat_rows, gate_matrix, up_matrix, down_matrix)  8.95 us
    slice x3, local copies, waits for them, and re-layouts, items_in_groups(): lax.slice_in_dim(a, low, high, axis=item_dim)  8.32 us
  transfers between devices with their start and end apart: 4, of which 4 were waited for; matrix products, arithmetic and copies ran while one was open for 30% of the time, Pallas kernels for 0%

commit v1 on v0

v1 whole, which is shorter than its diff:
```python
import jax
import jax.numpy as jnp
from jax import lax
from jax.experimental import pallas as pl
from jax.experimental.pallas import tpu as pltpu
from jax.sharding import PartitionSpec as P

eps_norm = 1e-05
MESH = pl.DeviceIdType.MESH

LINE = 4
SLOTS = 4
TOK = 32
CHUNK = 1024
CHUNKS = 3
ROWS = 256
FFE = 384
STRIDE = (7, 11, 13)


def iota(shape, dim):
    return lax.broadcasted_iota(jnp.int32, shape, dim)


def device(z, y, x, c):
    return ((z * 4 + y) * 4 + x) * 2 + c


def step_kernel(
    tok_ref, gain_ref, ids_ref, score_ref, prob_ref, gate_hbm, up_hbm, down_hbm,
    out_ref,
    w_in, w_out, xa, aux, sb, rb, xp, ob, gb, tsum, tb, fb, wm_hi, wm_lo,
    w_sem, s1, r1, sa, ra, s2, r2, s3, r3, s4, r4,
):
    me = lax.axis_index("ep")
    z, y, x, c = me // 32, (me // 8) % 4, (me // 2) % 4, me % 2
    other = 1 - c
    pos = (x, y, z)
    plane = ((z, y), (z, x), (x, y))

    def line_peer(q, p, core):
        return (
            device(z, y, p, core),
            device(z, p, x, core),
            device(p, y, x, core),
        )[q]

    def plane_peer(q, a, b, core):
        return (
            device(a, b, x, core),
            device(a, y, b, core),
            device(z, b, a, core),
        )[q]

    def rel(value, step):
        return (value + step) % 4

    weights = [
        pltpu.make_async_copy(gate_hbm.at[0], w_in.at[:, pl.ds(0, FFE)], w_sem.at[0]),
        pltpu.make_async_copy(up_hbm.at[0], w_in.at[:, pl.ds(FFE, FFE)], w_sem.at[1]),
        pltpu.make_async_copy(down_hbm.at[0], w_out, w_sem.at[2]),
    ]
    for copy in weights:
        copy.start()

    barrier = pltpu.get_barrier_semaphore()
    for q in range(CHUNKS):
        for step in range(1, LINE):
            for core in (c, other):
                pl.semaphore_signal(
                    barrier, inc=1, device_id=(line_peer(q, rel(pos[q], step), core),),
                    device_id_type=MESH,
                )
    pl.semaphore_signal(barrier, inc=1, device_id=(device(z, y, x, other),), device_id_type=MESH)

    values = tok_ref[...].astype(jnp.float32)
    centred = values - jnp.mean(values, axis=1, keepdims=True)
    variance = jnp.mean(centred * centred, axis=1, keepdims=True)
    normed = (centred * lax.rsqrt(variance + eps_norm) * gain_ref[...]).astype(jnp.bfloat16)
    for q in range(CHUNKS):
        xa[q, pl.ds(pos[q], 1)] = normed[:, q * CHUNK:(q + 1) * CHUNK][None]

    ids = ids_ref[...]
    scores = score_ref[...]
    exp_scores = jnp.exp(scores - jnp.max(scores, axis=1, keepdims=True))
    prob = jnp.sum(
        jnp.where(iota((TOK, TOK), 0) == iota((TOK, TOK), 1), prob_ref[...], 0.0),
        axis=1, keepdims=True,
    )
    mixing = exp_scores / jnp.sum(exp_scores, axis=1, keepdims=True) * prob
    lane = iota((TOK, 128), 1)
    matches = [ids[:, k:k + 1] == lane for k in range(4)]
    named = sum(jnp.where(match, 1.0, 0.0) for match in matches)
    earlier = jnp.where(iota((TOK, TOK), 1) < iota((TOK, TOK), 0), 1.0, 0.0)
    rank = jnp.dot(
        earlier.astype(jnp.bfloat16), named.astype(jnp.bfloat16),
        preferred_element_type=jnp.float32,
    )
    table = jnp.zeros((TOK, 128), jnp.float32)
    for k in range(4):
        slot = jnp.sum(jnp.where(matches[k], rank, 0.0), axis=1, keepdims=True)
        code = ids[:, k:k + 1].astype(jnp.float32) * 16.0 + slot
        table = jnp.where(lane == k, code, table)
        table = jnp.where(lane == 4 + k, mixing[:, k:k + 1], table)
    own_aux = jnp.transpose(jnp.concatenate([table] * 4, axis=0))[0:8]
    for q in range(CHUNKS):
        aux[q, pl.ds(pos[q], 1)] = own_aux[None]

    pl.semaphore_wait(barrier, 19)

    for step in (1, 3, 2):
        for q in range(CHUNKS):
            peer = (line_peer(q, rel(pos[q], step), c),)
            pltpu.make_async_remote_copy(
                src_ref=aux.at[q, pos[q]], dst_ref=aux.at[q, pos[q]],
                send_sem=sa.at[q], recv_sem=ra.at[q], device_id=peer, device_id_type=MESH,
            ).start()
            pltpu.make_async_remote_copy(
                src_ref=xa.at[q, pos[q]], dst_ref=xa.at[q, pos[q]],
                send_sem=s1.at[q], recv_sem=r1.at[q], device_id=peer, device_id_type=MESH,
            ).start()

    def bulk(ref, q, count, send_sem, recv_sem):
        part = ref.at[q, pl.ds(0, count)]
        return pltpu.make_async_remote_copy(
            src_ref=part, dst_ref=part, send_sem=send_sem, recv_sem=recv_sem,
            device_id=(me,), device_id_type=MESH,
        )

    def row_code(q, h, shape, dim):
        r = iota(shape, dim)
        a, b, low = r >> 6, (r >> 4) & 3, r & 15
        core = c if h == 0 else other
        return (plane_peer(q, a, b, core) * 16 + low).astype(jnp.float32)

    def line_aux(q):
        group = iota((8, 128), 1) >> 5
        found = jnp.zeros((8, 128), jnp.float32)
        for s in range(LINE):
            found = jnp.where(group == s, aux[q, s], found)
        return found + jnp.where(iota((8, 128), 0) < 4, (group * 4).astype(jnp.float32), 0.0)

    for q in range(CHUNKS):
        bulk(aux, q, LINE - 1, sa.at[q], ra.at[q]).wait_recv()
    found = [line_aux(q) for q in range(CHUNKS)]

    def pick(q, h):
        want = row_code(q, h, (ROWS, 128), 0)
        hit = found[q][0:1] == want
        for k in range(1, 4):
            hit = hit | (found[q][k:k + 1] == want)
        return jnp.where(hit, 1.0, 0.0).astype(jnp.bfloat16)

    def select(q, h):
        rows = jnp.dot(
            pick(q, h), xa[q].reshape(LINE * TOK, CHUNK), preferred_element_type=jnp.float32
        )
        sb[q, h * 16:(h + 1) * 16] = rows.astype(jnp.bfloat16).reshape(16, 16, CHUNK)

    def exchange(src, dst, h, send_sem, recv_sem):
        core = c if h == 0 else other

        def body(t, carry):
            for q in range(CHUNKS):
                turn = (t * STRIDE[q]) % 16
                a, b = rel(plane[q][0], turn // 4), rel(plane[q][1], turn % 4)
                pltpu.make_async_remote_copy(
                    src_ref=src.at[q, h * 16 + a * 4 + b],
                    dst_ref=dst.at[q, h * 16 + plane[q][0] * 4 + plane[q][1]],
                    send_sem=send_sem.at[h * 3 + q], recv_sem=recv_sem.at[h * 3 + q],
                    device_id=(plane_peer(q, a, b, core),), device_id_type=MESH,
                ).start()
            return carry

        lax.fori_loop(1 - h, 16, body, 0)
        if h == 0:
            for q in range(CHUNKS):
                mine = plane[q][0] * 4 + plane[q][1]
                dst[q, pl.ds(mine, 1)] = src[q, pl.ds(mine, 1)]

    for q in range(CHUNKS):
        bulk(xa, q, LINE - 1, s1.at[q], r1.at[q]).wait_recv()
        select(q, 0)
    exchange(sb, rb, 0, s2, r2)
    for q in range(CHUNKS):
        select(q, 1)
    exchange(sb, rb, 1, s2, r2)

    for q in range(CHUNKS):
        cols = jnp.transpose(
            jnp.concatenate([found[q], jnp.zeros((120, 128), jnp.float32)], axis=0)
        )
        for h in range(2):
            want = row_code(q, h, (128, ROWS), 1)
            scale = jnp.zeros((128, ROWS), jnp.float32)
            for k in range(4):
                scale = jnp.where(cols[:, k:k + 1] == want, cols[:, 4 + k:5 + k], scale)
            high = scale.astype(jnp.bfloat16)
            wm_hi[q, h] = high
            wm_lo[q, h] = (scale - high.astype(jnp.float32)).astype(jnp.bfloat16)

    def swap(high, low):
        i, j = iota((ROWS, ROWS), 0), iota((ROWS, ROWS), 1)
        rest = 255 - (3 << high) - (3 << low)
        moved = (i & rest) | (((i >> high) & 3) << low) | (((i >> low) & 3) << high)
        return jnp.where(moved == j, 1.0, 0.0).astype(jnp.bfloat16)

    orders = (None, swap(4, 2), swap(6, 2))

    def in_order(q, rows):
        if q == 0:
            return rows
        return jnp.dot(orders[q], rows, preferred_element_type=jnp.float32).astype(jnp.bfloat16)

    for copy in weights:
        copy.wait()
    for h in range(2):
        for q in range(CHUNKS):
            bulk(rb, q, 15 + h, s2.at[h * 3 + q], r2.at[h * 3 + q]).wait_recv()
            rows = rb[q, h * 16:(h + 1) * 16].reshape(ROWS, CHUNK)
            xp[:, q * CHUNK:(q + 1) * CHUNK] = in_order(q, rows)
        acts = jnp.dot(xp[...], w_in[...], preferred_element_type=jnp.float32)
        gate_act, up_act = acts[:, :FFE], acts[:, FFE:]
        hidden = (gate_act * jax.nn.sigmoid(gate_act) * up_act).astype(jnp.bfloat16)
        for q in range(CHUNKS):
            made = jnp.dot(
                in_order(q, hidden), w_out[:, q * CHUNK:(q + 1) * CHUNK],
                preferred_element_type=jnp.float32,
            )
            ob[q, h * 16:(h + 1) * 16] = made.astype(jnp.bfloat16).reshape(16, 16, CHUNK)
        exchange(ob, gb, h, s3, r3)

    for h in range(2):
        for q in range(CHUNKS):
            bulk(gb, q, 15 + h, s3.at[h * 3 + q], r3.at[h * 3 + q]).wait_recv()
            rows = gb[q, h * 16:(h + 1) * 16].reshape(ROWS, CHUNK)
            part = jnp.dot(wm_hi[q, h], rows, preferred_element_type=jnp.float32)
            part += jnp.dot(wm_lo[q, h], rows, preferred_element_type=jnp.float32)
            if h == 0:
                tsum[q] = part.reshape(LINE, TOK, CHUNK)
            else:
                part = tsum[q] + part.reshape(LINE, TOK, CHUNK)
                tsum[q] = part
                tb[q] = part.astype(jnp.bfloat16)
                for step in (2, 1, 3):
                    there = rel(pos[q], step)
                    pltpu.make_async_remote_copy(
                        src_ref=tb.at[q, there], dst_ref=fb.at[q, pos[q]],
                        send_sem=s4.at[q], recv_sem=r4.at[q],
                        device_id=(line_peer(q, there, c),), device_id_type=MESH,
                    ).start()

    for q in range(CHUNKS):
        bulk(fb, q, LINE - 1, s4.at[q], r4.at[q]).wait_recv()
        total = tsum[q, pl.ds(pos[q], 1)][0]
        for step in range(1, LINE):
            total += fb[q, pl.ds(rel(pos[q], step), 1)][0].astype(jnp.float32)
        out_ref[:, q * CHUNK:(q + 1) * CHUNK] = total.astype(jnp.bfloat16)

    for q in range(CHUNKS):
        bulk(aux, q, LINE - 1, sa.at[q], ra.at[q]).wait_send()
        bulk(xa, q, LINE - 1, s1.at[q], r1.at[q]).wait_send()
        bulk(tb, q, LINE - 1, s4.at[q], r4.at[q]).wait_send()
        for h in range(2):
            bulk(sb, q, 15 + h, s2.at[h * 3 + q], r2.at[h * 3 + q]).wait_send()
            bulk(ob, q, 15 + h, s3.at[h * 3 + q], r3.at[h * 3 + q]).wait_send()


def local(
    tokens, norm_gain, expert_ids, expert_scores, group_prob, gate_weight, up_weight, down_weight
):
    vmem = pl.BlockSpec(memory_space=pltpu.VMEM)
    hbm = pl.BlockSpec(memory_space=pl.ANY)
    bf16, f32 = jnp.bfloat16, jnp.float32
    dma = pltpu.SemaphoreType.DMA
    rows = pltpu.VMEM((CHUNKS, 32, 16, CHUNK), bf16)
    line = (CHUNKS, LINE, TOK, CHUNK)
    return pl.pallas_call(
        step_kernel,
        out_shape=jax.ShapeDtypeStruct(tokens.shape, bf16),
        in_specs=[vmem] * 5 + [hbm] * 3,
        out_specs=vmem,
        scratch_shapes=[
            pltpu.VMEM((CHUNKS * CHUNK, 2 * FFE), bf16),
            pltpu.VMEM((FFE, CHUNKS * CHUNK), bf16),
            pltpu.VMEM(line, bf16),
            pltpu.VMEM((CHUNKS, LINE, 8, 128), f32),
            rows,
            rows,
            pltpu.VMEM((ROWS, CHUNKS * CHUNK), bf16),
            rows,
            rows,
            pltpu.VMEM(line, f32),
            pltpu.VMEM(line, bf16),
            pltpu.VMEM(line, bf16),
            pltpu.VMEM((CHUNKS, 2, 128, ROWS), bf16),
            pltpu.VMEM((CHUNKS, 2, 128, ROWS), bf16),
            dma((3,)),
            dma((3,)), dma((3,)),
            dma((3,)), dma((3,)),
            dma((6,)), dma((6,)),
            dma((6,)), dma((6,)),
            dma((3,)), dma((3,)),
        ],
        compiler_params=pltpu.CompilerParams(
            collective_id=0, has_side_effects=True, vmem_limit_bytes=60 * 2**20
        ),
        name="expert_step",
    )(
        tokens, norm_gain[None, :], expert_ids, expert_scores, group_prob[None, :],
        gate_weight, up_weight, down_weight,
    )


def solution(mesh):
    in_specs = (
        P("ep", None),
        P(),
        P("ep", None),
        P("ep", None),
        P("ep"),
        P("ep", None, None),
        P("ep", None, None),
        P("ep", None, None),
    )
    out_specs = P("ep", None)
    return jax.shard_map(local, mesh=mesh, in_specs=in_specs, out_specs=out_specs, check_vma=False)
```

time: 140 us -> 75.3 us (0.54)
  Pallas kernels: 0 us -> 70.8 us
  waiting for transfers between devices: 56.4 us -> 0 us
  starting transfers between devices: 28.3 us -> 0 us
  local copies, waits for them, and re-layouts: 31.4 us -> 4.34 us
  matrix products: 20 us -> 0 us
  other arithmetic: 3.36 us -> 0 us
    pallas_call x0 -> x1, Pallas kernels: none -> 70.8 us  [local(): pl.pallas_call(step_kernel, out_shape=jax.ShapeDtypeStruct(tokens.shape,...]
    all_to_all x4 -> x0, waiting for transfers between devices: 56.4 us -> none  [the longest x2 28.8 us: serve_rows(): lax.all_to_all(results, 'ep', split_axis=0, concat_axis=0, tiled=True)]
    all_to_all x4 -> x0, starting transfers between devices: 28.3 us -> none  [the longest x2 17.3 us: moved(): lax.all_to_all(group, axis, split_axis=split_dim, concat_axis=concat_dim,...]
    dot_general x6 -> x0, matrix products: 20 us -> none  [the longest x2 10.4 us: expert_rows(): jnp.dot(hidden, down_matrix, preferred_element_type=jnp.float32)]
    reshape x4 -> x0, local copies, waits for them, and re-layouts: 18.2 us -> none  [the longest x2 9.29 us: serve_rows(): flat_rows = received.reshape(-1, model_width)]
    slice x3 -> x0, local copies, waits for them, and re-layouts: 8.32 us -> none  [items_in_groups(): lax.slice_in_dim(a, low, high, axis=item_dim)]
    all_to_all x2 -> x0, local copies, waits for them, and re-layouts: 4.78 us -> none  [serve_rows(): lax.all_to_all(results, 'ep', split_axis=0, concat_axis=0, tiled=True)]
    unnamed x10 -> x3, local copies, waits for them, and re-layouts: 0.03 us -> 4.34 us
  transfers between devices with their start and end apart: 4 -> 0, of which waited for: 4 -> 0; matrix products, arithmetic and copies ran while one was open for 30% -> 0% of each run, Pallas kernels for 0% -> 0%
where the time goes in v1:
time: 75.3 us; the launch traced here: 75.1 us
  Pallas kernels  70.8 us (94%)
  local copies, waits for them, and re-layouts  4.34 us (6%)
    pallas_call x1, Pallas kernels, local(): pl.pallas_call(step_kernel, out_shape=jax.ShapeDtypeStruct(tokens.shape,...  70.8 us
    unnamed x3, local copies, waits for them, and re-layouts  4.34 us

profile of v1, /device:TPU:1, one launch (start us, length us, event | category | flops | bytes accessed | tf_op | source)
XLA Modules:
  0.0 75.1 jit_solution(13937693681554015365)
XLA Ops:
  0.0 1.4 %copy.9.ids_ref = s32[32,4]{1,0:T(8,128)} copy(s32[32,4]{0,1:T(4,128)} %param.10) | data formatting | bytes 1024 | tf_op args[2]
  1.4 1.4 %copy.10.score_ref = f32[32,4]{1,0:T(8,128)} copy(f32[32,4]{0,1:T(4,128)} %param.11) | data formatting | bytes 1024 | tf_op args[3]
  2.7 70.8 %expert_step.1 = bf16[32,3072]{1,0:T(8,128)(2,1)} custom-call(bf16[32,3072]{1,0:T(8,128)(2,1)} %tok_ref.1, f32[1,3072]{1,0:T(1,128)} %bitcast.2, s32[32,4]{1,0:T(8,128)} %copy.9.ids_ref, f32[32,4]{1,0:T(8,128)} %copy.10.score_ref, f32[1,32]{1,0:T(1,128)} %bitcast.3, bf16[1,3072,384]{2,1,0:T(8,128)(2,1)} %gate_hbm.1, bf16[1,3072,384]{2,1,0:T(8,128)(2,1)} %up_hbm.1, ...), custom_call_target="tpu_custom_call" | custom-call | tf_op jit(solution)/shard_map/expert_step/pallas_call | solution.py:278
  73.5 1.6 %copy.12 = bf16[32,3072]{1,0:T(8,128)(2,1)} copy(bf16[32,3072]{1,0:T(8,128)(2,1)} %expert_step.1) | data formatting | bytes 393216

commit v2 on v1

v2 whole, which is shorter than its diff:
```python
import jax
import jax.numpy as jnp
from jax import lax
from jax.experimental import pallas as pl
from jax.experimental.pallas import tpu as pltpu
from jax.sharding import PartitionSpec as P

eps_norm = 1e-05
MESH = pl.DeviceIdType.MESH

LINE = 4
SLOTS = 4
TOK = 32
KINDS = 3
CHUNK = 512
CHUNKS = 6
PARTS = ((0, 1, 2), (3, 4, 5))
ROWS = 256
FFE = 384
STRIDE = (7, 11, 13)


def iota(shape, dim):
    return lax.broadcasted_iota(jnp.int32, shape, dim)


def device(z, y, x, c):
    return ((z * 4 + y) * 4 + x) * 2 + c


def columns(j):
    return slice(j * CHUNK, (j + 1) * CHUNK)


def step_kernel(
    tok_hbm, gain_hbm, ids_hbm, score_hbm, prob_hbm, gate_hbm, up_hbm, down_hbm,
    parts_ref,
    tok_ref, gain_ref, ids_ref, score_ref, prob_ref, spread,
    w_in, w_out, xa, aux, picks, sb, rb, xp, ob, gb, tsum, tb, wm_hi, wm_lo,
    in_sem, w_sem, own_sem, s1, r1, sa, ra, s2, r2, s3, r3, s4, r4,
):
    me = lax.axis_index("ep")
    z, y, x, c = me // 32, (me // 8) % 4, (me // 2) % 4, me % 2
    other = 1 - c
    pos = (x, y, z)
    plane = ((z, y), (z, x), (x, y))

    def line_peer(q, p, core):
        return (
            device(z, y, p, core),
            device(z, p, x, core),
            device(p, y, x, core),
        )[q]

    def plane_peer(q, a, b, core):
        return (
            device(a, b, x, core),
            device(a, y, b, core),
            device(z, b, a, core),
        )[q]

    def rel(value, step):
        return (value + step) % 4

    barrier = pltpu.get_barrier_semaphore()
    for q in range(KINDS):
        for step in range(1, LINE):
            for core in (c, other):
                pl.semaphore_signal(
                    barrier, inc=1, device_id=(line_peer(q, rel(pos[q], step), core),),
                    device_id_type=MESH,
                )
    pl.semaphore_signal(barrier, inc=1, device_id=(device(z, y, x, other),), device_id_type=MESH)

    smalls = [
        pltpu.make_async_copy(src, dst, in_sem.at[i])
        for i, (src, dst) in enumerate((
            (tok_hbm, tok_ref), (gain_hbm, gain_ref), (ids_hbm, ids_ref),
            (score_hbm, score_ref), (prob_hbm, prob_ref),
        ))
    ]
    for copy in smalls:
        copy.start()
    weights = [
        pltpu.make_async_copy(gate_hbm.at[0], w_in.at[:, pl.ds(0, FFE)], w_sem.at[0]),
        pltpu.make_async_copy(up_hbm.at[0], w_in.at[:, pl.ds(FFE, FFE)], w_sem.at[1]),
        pltpu.make_async_copy(down_hbm.at[0], w_out, w_sem.at[2]),
    ]
    for copy in weights:
        copy.start()
    for copy in smalls:
        copy.wait()

    ids = ids_ref[...]
    scores = score_ref[...]
    exp_scores = jnp.exp(scores - jnp.max(scores, axis=0, keepdims=True))
    mixing = exp_scores / jnp.sum(exp_scores, axis=0, keepdims=True) * prob_ref[...]
    expert = iota((128, TOK), 0)
    matches = [ids[k:k + 1] == expert for k in range(4)]
    named = sum(jnp.where(match, 1.0, 0.0) for match in matches)
    earlier = jnp.where(iota((TOK, TOK), 0) < iota((TOK, TOK), 1), 1.0, 0.0)
    rank = jnp.dot(
        named.astype(jnp.bfloat16), earlier.astype(jnp.bfloat16),
        preferred_element_type=jnp.float32,
    )
    spread[...] = jnp.zeros((8, 128), jnp.float32)
    for k in range(4):
        slot = jnp.sum(jnp.where(matches[k], rank, 0.0), axis=0, keepdims=True)
        spread[k:k + 1, 0:TOK] = ids[k:k + 1].astype(jnp.float32) * 16.0 + slot
        spread[4 + k:5 + k, 0:TOK] = mixing[k:k + 1]
    own_aux = spread[...]
    own_aux = own_aux + pltpu.roll(own_aux, TOK, 1)
    own_aux = own_aux + pltpu.roll(own_aux, 2 * TOK, 1)
    for q in range(KINDS):
        aux[q, pl.ds(pos[q], 1)] = own_aux[None]

    values = tok_ref[...].astype(jnp.float32)
    average = jnp.mean(values, axis=1, keepdims=True)
    centred = values - average
    scale = lax.rsqrt(jnp.mean(centred * centred, axis=1, keepdims=True) + eps_norm)

    def normalise(part):
        for j in part:
            values = tok_ref[:, columns(j)].astype(jnp.float32)
            normed = (values - average) * scale * gain_ref[:, columns(j)]
            xa[j, pl.ds(pos[j % 3], 1)] = normed.astype(jnp.bfloat16)[None]

    def gather(part):
        for step in (2, 1, 3):
            for j in part:
                q = j % 3
                pltpu.make_async_remote_copy(
                    src_ref=xa.at[j, pos[q]], dst_ref=xa.at[j, pos[q]],
                    send_sem=s1.at[j], recv_sem=r1.at[j],
                    device_id=(line_peer(q, rel(pos[q], step), c),), device_id_type=MESH,
                ).start()

    normalise(PARTS[0])
    pl.semaphore_wait(barrier, 19)
    for step in (2, 1, 3):
        for q in range(KINDS):
            pltpu.make_async_remote_copy(
                src_ref=aux.at[q, pos[q]], dst_ref=aux.at[q, pos[q]],
                send_sem=sa.at[q], recv_sem=ra.at[q],
                device_id=(line_peer(q, rel(pos[q], step), c),), device_id_type=MESH,
            ).start()
    gather(PARTS[0])
    normalise(PARTS[1])
    gather(PARTS[1])

    def bulk(ref, j, count, send_sem, recv_sem):
        part = ref.at[j, pl.ds(0, count)]
        return pltpu.make_async_remote_copy(
            src_ref=part, dst_ref=part, send_sem=send_sem, recv_sem=recv_sem,
            device_id=(me,), device_id_type=MESH,
        )

    def row_code(q, h, shape, dim):
        r = iota(shape, dim)
        a, b, low = r >> 6, (r >> 4) & 3, r & 15
        core = c if h == 0 else other
        return (plane_peer(q, a, b, core) * 16 + low).astype(jnp.float32)

    def line_aux(q):
        group = iota((8, 128), 1) >> 5
        found = jnp.zeros((8, 128), jnp.float32)
        for s in range(LINE):
            found = jnp.where(group == s, aux[q, s], found)
        return found + jnp.where(iota((8, 128), 0) < 4, (group * 4).astype(jnp.float32), 0.0)

    for q in range(KINDS):
        bulk(aux, q, LINE - 1, sa.at[q], ra.at[q]).wait_recv()
    found = [line_aux(q) for q in range(KINDS)]
    for h in range(2):
        for q in range(KINDS):
            want = row_code(q, h, (ROWS, 128), 0)
            hit = found[q][0:1] == want
            for k in range(1, 4):
                hit = hit | (found[q][k:k + 1] == want)
            picks[q, h] = jnp.where(hit, 1.0, 0.0).astype(jnp.bfloat16)

    def exchange(src, dst, h, part, send_sem, recv_sem):
        core = c if h == 0 else other

        def body(t, carry):
            for j in part:
                q = j % 3
                turn = (t * STRIDE[q]) % 16
                a, b = rel(plane[q][0], turn // 4), rel(plane[q][1], turn % 4)
                pltpu.make_async_remote_copy(
                    src_ref=src.at[j, h * 16 + a * 4 + b],
                    dst_ref=dst.at[j, h * 16 + plane[q][0] * 4 + plane[q][1]],
                    send_sem=send_sem.at[h * CHUNKS + j], recv_sem=recv_sem.at[h * CHUNKS + j],
                    device_id=(plane_peer(q, a, b, core),), device_id_type=MESH,
                ).start()
            return carry

        lax.fori_loop(1 - h, 16, body, 0)
        if h == 0:
            for j in part:
                mine = plane[j % 3][0] * 4 + plane[j % 3][1]
                dst[j, pl.ds(mine, 1)] = src[j, pl.ds(mine, 1)]

    for h in range(2):
        for part in PARTS:
            for j in part:
                if h == 0:
                    bulk(xa, j, LINE - 1, s1.at[j], r1.at[j]).wait_recv()
                rows = jnp.dot(
                    picks[j % 3, h], xa[j].reshape(LINE * TOK, CHUNK),
                    preferred_element_type=jnp.float32,
                )
                sb[j, h * 16:(h + 1) * 16] = rows.astype(jnp.bfloat16).reshape(16, 16, CHUNK)
            exchange(sb, rb, h, part, s2, r2)

    for q in range(KINDS):
        cols = jnp.transpose(
            jnp.concatenate([found[q], jnp.zeros((120, 128), jnp.float32)], axis=0)
        )
        for h in range(2):
            want = row_code(q, h, (128, ROWS), 1)
            factor = jnp.zeros((128, ROWS), jnp.float32)
            for k in range(4):
                factor = jnp.where(cols[:, k:k + 1] == want, cols[:, 4 + k:5 + k], factor)
            high = factor.astype(jnp.bfloat16)
            wm_hi[q, h] = high
            wm_lo[q, h] = (factor - high.astype(jnp.float32)).astype(jnp.bfloat16)

    def swap(high, low):
        i, j = iota((ROWS, ROWS), 0), iota((ROWS, ROWS), 1)
        rest = 255 - (3 << high) - (3 << low)
        moved = (i & rest) | (((i >> high) & 3) << low) | (((i >> low) & 3) << high)
        return jnp.where(moved == j, 1.0, 0.0).astype(jnp.bfloat16)

    orders = (None, swap(4, 2), swap(6, 2))

    def in_order(q, rows):
        if q == 0:
            return rows
        return jnp.dot(orders[q], rows, preferred_element_type=jnp.float32).astype(jnp.bfloat16)

    for copy in weights:
        copy.wait()
    for h in range(2):
        for j in range(CHUNKS):
            i = h * CHUNKS + j
            bulk(rb, j, 15 + h, s2.at[i], r2.at[i]).wait_recv()
            rows = rb[j, h * 16:(h + 1) * 16].reshape(ROWS, CHUNK)
            xp[:, columns(j)] = in_order(j % 3, rows)
        acts = jnp.dot(xp[...], w_in[...], preferred_element_type=jnp.float32)
        gate_act, up_act = acts[:, :FFE], acts[:, FFE:]
        hidden = (gate_act * jax.nn.sigmoid(gate_act) * up_act).astype(jnp.bfloat16)
        hidden = [in_order(q, hidden) for q in range(KINDS)]
        for part in PARTS:
            for j in part:
                made = jnp.dot(hidden[j % 3], w_out[:, columns(j)], preferred_element_type=jnp.float32)
                ob[j, h * 16:(h + 1) * 16] = made.astype(jnp.bfloat16).reshape(16, 16, CHUNK)
            exchange(ob, gb, h, part, s3, r3)

    def here(q, j):
        return parts_ref.at[pos[q], :, pl.ds(j * CHUNK, CHUNK)]

    for h in range(2):
        for j in range(CHUNKS):
            q, i = j % 3, h * CHUNKS + j
            bulk(gb, j, 15 + h, s3.at[i], r3.at[i]).wait_recv()
            rows = gb[j, h * 16:(h + 1) * 16].reshape(ROWS, CHUNK)
            part = jnp.dot(wm_hi[q, h], rows, preferred_element_type=jnp.float32)
            part += jnp.dot(wm_lo[q, h], rows, preferred_element_type=jnp.float32)
            if h == 0:
                tsum[j] = part
            else:
                tb[j] = (tsum[j] + part).astype(jnp.bfloat16).reshape(LINE, TOK, CHUNK)
                for step in (2, 1, 3):
                    there = rel(pos[q], step)
                    pltpu.make_async_remote_copy(
                        src_ref=tb.at[j, there], dst_ref=here(q, j),
                        send_sem=s4.at[j], recv_sem=r4.at[j],
                        device_id=(line_peer(q, there, c),), device_id_type=MESH,
                    ).start()
                pltpu.make_async_copy(tb.at[j, pos[q]], here(q, j), own_sem.at[j]).start()

    for j in range(CHUNKS):
        q = j % 3
        bulk(xa, j, LINE - 1, s1.at[j], r1.at[j]).wait_send()
        for h in range(2):
            i = h * CHUNKS + j
            bulk(sb, j, 15 + h, s2.at[i], r2.at[i]).wait_send()
            bulk(ob, j, 15 + h, s3.at[i], r3.at[i]).wait_send()
    for q in range(KINDS):
        bulk(aux, q, LINE - 1, sa.at[q], ra.at[q]).wait_send()
    for j in range(CHUNKS):
        q = j % 3
        pltpu.make_async_copy(tb.at[j, pos[q]], here(q, j), own_sem.at[j]).wait()
        bulk(tb, j, LINE - 1, s4.at[j], r4.at[j]).wait()


def local(
    tokens, norm_gain, expert_ids, expert_scores, group_prob, gate_weight, up_weight, down_weight
):
    hbm = pl.BlockSpec(memory_space=pl.ANY)
    bf16, f32 = jnp.bfloat16, jnp.float32
    dma = pltpu.SemaphoreType.DMA
    width = CHUNKS * CHUNK
    rows = pltpu.VMEM((CHUNKS, 32, 16, CHUNK), bf16)
    line = (CHUNKS, LINE, TOK, CHUNK)
    parts = pl.pallas_call(
        step_kernel,
        out_shape=jax.ShapeDtypeStruct((LINE, TOK, width), bf16),
        in_specs=[hbm] * 8,
        out_specs=hbm,
        scratch_shapes=[
            pltpu.VMEM((TOK, width), bf16),
            pltpu.VMEM((1, width), f32),
            pltpu.VMEM((4, TOK), jnp.int32),
            pltpu.VMEM((4, TOK), f32),
            pltpu.VMEM((1, TOK), f32),
            pltpu.VMEM((8, 128), f32),
            pltpu.VMEM((width, 2 * FFE), bf16),
            pltpu.VMEM((FFE, width), bf16),
            pltpu.VMEM(line, bf16),
            pltpu.VMEM((KINDS, LINE, 8, 128), f32),
            pltpu.VMEM((KINDS, 2, ROWS, 128), bf16),
            rows,
            rows,
            pltpu.VMEM((ROWS, width), bf16),
            rows,
            rows,
            pltpu.VMEM((CHUNKS, LINE * TOK, CHUNK), f32),
            pltpu.VMEM(line, bf16),
            pltpu.VMEM((KINDS, 2, 128, ROWS), bf16),
            pltpu.VMEM((KINDS, 2, 128, ROWS), bf16),
            dma((5,)), dma((3,)), dma((6,)),
            dma((6,)), dma((6,)),
            dma((3,)), dma((3,)),
            dma((12,)), dma((12,)),
            dma((12,)), dma((12,)),
            dma((6,)), dma((6,)),
        ],
        compiler_params=pltpu.CompilerParams(
            collective_id=0, has_side_effects=True, vmem_limit_bytes=60 * 2**20
        ),
        name="expert_step",
    )(
        tokens, norm_gain[None, :], expert_ids.T, expert_scores.T, group_prob[None, :],
        gate_weight, up_weight, down_weight,
    )
    terms = [parts[s].astype(f32) for s in range(LINE)]
    return ((terms[0] + terms[1]) + (terms[2] + terms[3])).astype(bf16)


def solution(mesh):
    in_specs = (
        P("ep", None),
        P(),
        P("ep", None),
        P("ep", None),
        P("ep"),
        P("ep", None, None),
        P("ep", None, None),
        P("ep", None, None),
    )
    out_specs = P("ep", None)
    return jax.shard_map(local, mesh=mesh, in_specs=in_specs, out_specs=out_specs, check_vma=False)
```

time: 75.3 us -> 67.5 us (0.90)
  Pallas kernels: 70.8 us -> 65.3 us
  local copies, waits for them, and re-layouts: 4.34 us -> 0 us
  other arithmetic: 0 us -> 2 us
    pallas_call x1, Pallas kernels: 70.8 us -> 65.3 us  [local(): pl.pallas_call(step_kernel, out_shape=jax.ShapeDtypeStruct((LINE, TOK, wi...]
    unnamed x3 -> x0, local copies, waits for them, and re-layouts: 4.34 us -> none
    convert_element_type x0 -> x1, other arithmetic: none -> 2 us  [local(): return (terms[0] + terms[1] + (terms[2] + terms[3])).astype(bf16)]
where the time goes in v2:
time: 67.5 us; the launch traced here: 67.4 us
  Pallas kernels  65.3 us (97%)
  other arithmetic  2 us (3%)
    pallas_call x1, Pallas kernels, local(): pl.pallas_call(step_kernel, out_shape=jax.ShapeDtypeStruct((LINE, TOK, wi...  65.3 us
    convert_element_type x1, other arithmetic, local(): return (terms[0] + terms[1] + (terms[2] + terms[3])).astype(bf16)  2 us

profile of v2, /device:TPU:1, one launch (start us, length us, event | category | flops | bytes accessed | tf_op | source)
XLA Modules:
  0.0 67.4 jit_solution(10404303469240215562)
XLA Ops:
  0.0 65.3 %expert_step.1 = bf16[4,32,3072]{2,1,0:T(8,128)(2,1)} custom-call(bf16[32,3072]{1,0:T(8,128)(2,1)} %tok_hbm.1, f32[1,3072]{1,0:T(1,128)} %bitcast.6, s32[4,32]{1,0:T(4,128)} %bitcast.7, f32[4,32]{1,0:T(4,128)} %bitcast.8, f32[1,32]{1,0:T(1,128)} %bitcast.9, bf16[1,3072,384]{2,1,0:T(8,128)(2,1)} %gate_hbm.1, bf16[1,3072,384]{2,1,0:T(8,128)(2,1)} %up_hbm.1, ...), custom_call_target="tpu_custom_call" | custom-call | tf_op jit(solution)/shard_map/expert_step/pallas_call | solution.py:307
  65.4 2.0 %fusion = bf16[32,3072]{1,0:T(8,128)(2,1)} fusion(bf16[4,32,3072]{2,1,0:T(8,128)(2,1)} %expert_step.1), kind=kLoop, calls=%fused_computation.1 | loop fusion | flops 786432 | bytes 983040 | tf_op jit(solution)/shard_map/convert_element_type | solution.py:349

commit v3 on v2

v3 whole, which is shorter than its diff:
```python
import jax
import jax.numpy as jnp
from jax import lax
from jax.experimental import pallas as pl
from jax.experimental.pallas import tpu as pltpu
from jax.sharding import PartitionSpec as P

eps_norm = 1e-05
MESH = pl.DeviceIdType.MESH

LINE = 4
TOK = 32
CHUNK = 1024
CHUNKS = 3
PIECE = 512
PIECES = 6
PARTS = ((0, 1, 2), (3, 4, 5))
ROWS = 256
FFE = 384
STRIDE = (7, 11, 13)
FAR = (10, 9, 6, 11, 14, 8, 2, 5, 7, 13, 15, 4, 1, 12, 3, 0)


def iota(shape, dim):
    return lax.broadcasted_iota(jnp.int32, shape, dim)


def one_hot(hit):
    return jnp.where(hit, 1.0, 0.0).astype(jnp.bfloat16)


def device(z, y, x, c):
    return ((z * 4 + y) * 4 + x) * 2 + c


def columns(j):
    low = (j % 3) * CHUNK + (j // 3) * PIECE
    return slice(low, low + PIECE)


def step_kernel(
    tok_hbm, gain_hbm, ids_hbm, score_hbm, prob_hbm, gate_hbm, up_hbm, down_hbm,
    parts_ref,
    tok_ref, gain_ref, ids_ref, score_ref, prob_ref, spread,
    w_in, w_out, xa, aux, codes, sb, rb, xp, ob, gb, tsum, tb, wm,
    in_sem, w_sem, own_sem, s1, r1, sa, ra, sl, rl, sn, rn, s2, r2, s3, r3, s4, r4,
):
    me = lax.axis_index("ep")
    z, y, x, c = me // 32, (me // 8) % 4, (me // 2) % 4, me % 2
    other = 1 - c
    pos = (x, y, z)
    plane = ((z, y), (z, x), (x, y))

    def rel(value, step):
        return (value + step) % 4

    def line_peer(q, step, core):
        p = rel(pos[q], step)
        return (
            device(z, y, p, core),
            device(z, p, x, core),
            device(p, y, x, core),
        )[q]

    def plane_peer(q, a, b, core):
        return (
            device(a, b, x, core),
            device(a, y, b, core),
            device(z, b, a, core),
        )[q]

    smalls = [
        pltpu.make_async_copy(src, dst, in_sem.at[i])
        for i, (src, dst) in enumerate((
            (tok_hbm, tok_ref), (gain_hbm, gain_ref), (ids_hbm, ids_ref),
            (score_hbm, score_ref), (prob_hbm, prob_ref),
        ))
    ]
    for copy in smalls:
        copy.start()
    weights = [
        pltpu.make_async_copy(gate_hbm.at[0], w_in.at[:, pl.ds(0, FFE)], w_sem.at[0]),
        pltpu.make_async_copy(up_hbm.at[0], w_in.at[:, pl.ds(FFE, FFE)], w_sem.at[1]),
        pltpu.make_async_copy(down_hbm.at[0], w_out, w_sem.at[2]),
    ]
    for copy in weights:
        copy.start()
    barrier = pltpu.get_barrier_semaphore()
    for step in (2, 1, 3):
        for q in range(CHUNKS):
            for core in (c, other):
                pl.semaphore_signal(
                    barrier, inc=1, device_id=(line_peer(q, step, core),), device_id_type=MESH
                )
    pl.semaphore_signal(barrier, inc=1, device_id=(device(z, y, x, other),), device_id_type=MESH)

    for copy in smalls[:2]:
        copy.wait()

    values = tok_ref[...].astype(jnp.float32)
    centred = values - jnp.mean(values, axis=1, keepdims=True)
    variance = jnp.mean(centred * centred, axis=1, keepdims=True)
    normed = (centred * lax.rsqrt(variance + eps_norm) * gain_ref[...]).astype(jnp.bfloat16)
    for q in range(CHUNKS):
        xa[q, 0, 0] = normed[:, q * CHUNK:(q + 1) * CHUNK]

    def send(src, dst, send_sem, recv_sem, peer):
        pltpu.make_async_remote_copy(
            src_ref=src, dst_ref=dst, send_sem=send_sem, recv_sem=recv_sem,
            device_id=(peer,), device_id_type=MESH,
        ).start()

    def to_neighbours(q, d):
        for step in (1, 3):
            send(
                xa.at[q, 0, d], xa.at[q, 4 - step, d], sn.at[q, step, d], rn.at[q, 4 - step, d],
                line_peer((q + 1) % 3, step, c),
            )

    for copy in smalls[2:]:
        copy.wait()
    ids = ids_ref[...]
    scores = score_ref[...]
    exp_scores = jnp.exp(scores - jnp.max(scores, axis=0, keepdims=True))
    mixing = exp_scores / jnp.sum(exp_scores, axis=0, keepdims=True) * prob_ref[...]
    expert = iota((128, TOK), 0)
    matches = [ids[k:k + 1] == expert for k in range(4)]
    named = sum(jnp.where(match, 1.0, 0.0) for match in matches)
    earlier = jnp.where(iota((TOK, TOK), 0) < iota((TOK, TOK), 1), 1.0, 0.0)
    rank = jnp.dot(
        named.astype(jnp.bfloat16), earlier.astype(jnp.bfloat16),
        preferred_element_type=jnp.float32,
    )
    spread[...] = jnp.zeros((8, 128), jnp.float32)
    for k in range(4):
        slot = jnp.sum(jnp.where(matches[k], rank, 0.0), axis=0, keepdims=True)
        spread[k:k + 1, 0:TOK] = ids[k:k + 1].astype(jnp.float32) * 16.0 + slot
        spread[4 + k:5 + k, 0:TOK] = mixing[k:k + 1]
    own = spread[...]
    own = own + pltpu.roll(own, TOK, 1)
    own = own + pltpu.roll(own, 2 * TOK, 1)
    quarter = ((iota((8, 128), 1) >> 5) * 4).astype(jnp.float32)
    own = own + jnp.where(iota((8, 128), 0) < 4, quarter, 0.0)
    for q in range(CHUNKS):
        aux[q, 0] = own

    pl.semaphore_wait(barrier, 19)
    for step in (2, 1, 3):
        for q in range(CHUNKS):
            send(
                aux.at[q, 0], aux.at[q, 4 - step], sa.at[q, step], ra.at[q, 4 - step],
                line_peer(q, step, c),
            )
    for step in (2, 1, 3):
        for q in range(CHUNKS):
            send(
                xa.at[q, 0, 0], xa.at[q, 0, 4 - step], s1.at[q, step], r1.at[q, 4 - step],
                line_peer(q, step, c),
            )
    for q in range(CHUNKS):
        to_neighbours(q, 0)

    def whole(ref, send_sem, recv_sem):
        return pltpu.make_async_remote_copy(
            src_ref=ref, dst_ref=ref, send_sem=send_sem, recv_sem=recv_sem,
            device_id=(me,), device_id_type=MESH,
        )

    def bulk(ref, j, h, low, width, send_sem, recv_sem):
        part = ref.at[j, pl.ds(0, 15 + h), :, pl.ds(low, width)]
        i = (1 + h) if low else h
        return whole(part, send_sem.at[i, j], recv_sem.at[i, j])

    def row_code(q, h, shape, dim):
        r = iota(shape, dim)
        a, b, low = r >> 6, (r >> 4) & 3, r & 15
        core = c if h == 0 else other
        return (plane_peer(q, a, b, core) * 16 + low).astype(jnp.float32)

    def exchange(h, part, low=0, width=PIECE):
        core = c if h == 0 else other

        def body(t, carry):
            for j in part:
                q = j % 3
                turn = t if low else (t * STRIDE[q]) % 16
                a, b = rel(plane[q][0], turn // 4), rel(plane[q][1], turn % 4)
                i = (1 + h) if low else h
                send(
                    ob.at[j, h * 16 + a * 4 + b, :, pl.ds(low, width)],
                    gb.at[j, h * 16 + plane[q][0] * 4 + plane[q][1], :, pl.ds(low, width)],
                    s3.at[i, j], r3.at[i, j], plane_peer(q, a, b, core),
                )
            return carry

        if low:
            for t in FAR:
                body(t, 0)
        else:
            lax.fori_loop(1 - h, 16, body, 0)
        if h == 0:
            for j in part:
                mine = plane[j % 3][0] * 4 + plane[j % 3][1]
                gb[j, pl.ds(mine, 1)] = ob[j, pl.ds(mine, 1)]

    for q in range(CHUNKS):
        for d in (1, 3, 2):
            whole(aux.at[q, d], sa.at[q, d], ra.at[q, d]).wait_recv()
    group = iota((8, 128), 1) >> 5
    for q in range(CHUNKS):
        found = aux[q, 0]
        for d in range(1, LINE):
            found = jnp.where(group == d, aux[q, d], found)
        codes[q, 0] = found
    for step in (2, 1, 3):
        for q in range(CHUNKS):
            send(
                codes.at[q, 0], codes.at[q, 4 - step], sl.at[q, step], rl.at[q, 4 - step],
                line_peer((q + 1) % 3, step, c),
            )
    for d in (1, 3, 2):
        for q in range(CHUNKS):
            whole(xa.at[q, 0, d], s1.at[q, d], r1.at[q, d]).wait_recv()
            to_neighbours(q, d)

    half = CHUNK // 2

    def select(e):
        for q in range(CHUNKS):
            r = iota((128, 128), 0)
            h, step = r >> 6, (r >> 4) & 3
            core = c + h - 2 * c * h
            want = (line_peer((q + 2) % 3, step, core) * 16 + (r & 15)).astype(jnp.float32)
            found = codes[q, e]
            hit = found[0:1] == want
            for k in range(1, 4):
                hit = hit | (found[k:k + 1] == want)
            rows = jnp.dot(
                one_hot(hit), xa[q, e].reshape(LINE * TOK, CHUNK),
                preferred_element_type=jnp.float32,
            )
            sb[q, e] = rows.astype(jnp.bfloat16).reshape(2, LINE, 16, CHUNK)

    def deliver(h, e):
        core = c if h == 0 else other
        for step in (2, 1, 3, 0):
            for q in range(CHUNKS):
                if h == 0 and step == 0:
                    rb[q, 0, 0, e] = sb[q, e, 0, 0]
                    continue
                for low in (0, half):
                    send(
                        sb.at[q, e, h, step, :, pl.ds(low, half)],
                        rb.at[q, h, (4 - step) % 4, e, :, pl.ds(low, half)],
                        s2.at[q, h], r2.at[q, h], line_peer((q + 2) % 3, step, core),
                    )

    select(0)
    deliver(0, 0)
    for d in (0, 1, 3, 2):
        for q in range(CHUNKS):
            for step, low in ((3, 0), (1, half)):
                e = 4 - step
                whole(xa.at[q, e, d], sn.at[q, e, d], rn.at[q, e, d]).wait_recv()
                send(
                    xa.at[q, e, d, :, pl.ds(low, half)], xa.at[q, 2, d, :, pl.ds(low, half)],
                    sn.at[q, 2, 0], rn.at[q, 2, 0], line_peer((q + 1) % 3, step, c),
                )
    for q in range(CHUNKS):
        for e in (1, 3, 2):
            whole(codes.at[q, e], sl.at[q, e], rl.at[q, e]).wait_recv()
    for e in (1, 3):
        select(e)
        deliver(0, e)
    for q in range(CHUNKS):
        whole(xa.at[q, 2], sn.at[q, 2, 0], rn.at[q, 2, 0]).wait_recv()
    select(2)
    deliver(0, 2)
    for e in (0, 1, 3, 2):
        deliver(1, e)

    for q in range(CHUNKS):
        cols = jnp.transpose(
            jnp.concatenate([codes[q, 0], jnp.zeros((120, 128), jnp.float32)], axis=0)
        )
        for h in range(2):
            want = row_code(q, h, (128, ROWS), 1)
            factor = jnp.zeros((128, ROWS), jnp.float32)
            for k in range(4):
                factor = jnp.where(cols[:, k:k + 1] == want, cols[:, 4 + k:5 + k], factor)
            high = factor.astype(jnp.bfloat16)
            wm[q, h, 0:128] = high
            wm[q, h, 128:256] = (factor - high.astype(jnp.float32)).astype(jnp.bfloat16)

    square = (ROWS, ROWS)

    def arrived(q, o):
        zz, yy, xx, slot = o >> 6, (o >> 4) & 3, (o >> 2) & 3, o & 3
        if q == 1:
            return xx * 64 + zz * 16 + yy * 4 + slot
        return yy * 64 + xx * 16 + zz * 4 + slot

    def leaving(q, o):
        zz, yy, xx, slot = o >> 6, (o >> 4) & 3, (o >> 2) & 3, o & 3
        az, ay, ax = (zz + z) & 3, (yy + y) & 3, (xx + x) & 3
        if q == 0:
            return az * 64 + ay * 16 + xx * 4 + slot
        if q == 1:
            return az * 64 + ax * 16 + yy * 4 + slot
        return ax * 64 + ay * 16 + zz * 4 + slot

    gather_order = [None] + [
        one_hot(arrived(q, iota(square, 0)) == iota(square, 1)) for q in (1, 2)
    ]
    spread_order = [
        one_hot(leaving(q, iota(square, 1)) == iota(square, 0)) for q in range(CHUNKS)
    ]

    def ordered(order, rows):
        if order is None:
            return rows
        return jnp.dot(order, rows, preferred_element_type=jnp.float32).astype(jnp.bfloat16)

    for copy in weights:
        copy.wait()
    for h in range(2):
        for q in range(CHUNKS):
            part = rb.at[q, h] if h else rb.at[q, 0, pl.ds(0, 3)]
            whole(part, s2.at[q, h], r2.at[q, h]).wait_recv()
            rows = rb[q, h].reshape(ROWS, CHUNK)
            xp[:, q * CHUNK:(q + 1) * CHUNK] = ordered(gather_order[q], rows)
        acts = jnp.dot(xp[...], w_in[...], preferred_element_type=jnp.float32)
        gate_act, up_act = acts[:, :FFE], acts[:, FFE:]
        hidden = (gate_act * jax.nn.sigmoid(gate_act) * up_act).astype(jnp.bfloat16)
        hidden = [ordered(spread_order[q], hidden) for q in range(CHUNKS)]
        for part in PARTS:
            for j in part:
                made = jnp.dot(
                    hidden[j % 3], w_out[:, columns(j)], preferred_element_type=jnp.float32
                )
                ob[j, h * 16:(h + 1) * 16] = made.astype(jnp.bfloat16).reshape(16, 16, PIECE)
            if h == 1 and part is PARTS[1]:
                exchange(1, part, 0, PIECE // 2)
                exchange(1, part, PIECE // 2, PIECE // 2)
            else:
                exchange(h, part)

    def here(j, slot, low, width):
        return parts_ref.at[slot, :, pl.ds(columns(j).start + low, width)]

    def summed(j, h, low, width):
        bulk(gb, j, h, low, width, s3, r3).wait_recv()
        rows = gb[j, h * 16:(h + 1) * 16, :, low:low + width].reshape(ROWS, width)
        both = jnp.dot(wm[j % 3, h], rows, preferred_element_type=jnp.float32)
        return both[0:128] + both[128:256]

    def settle(j, low, width):
        q = j % 3
        total = tsum[j, :, low:low + width] + summed(j, 1, low, width)
        tb[j, :, :, low:low + width] = total.astype(jnp.bfloat16).reshape(LINE, TOK, width)
        i = 1 if low else 0
        for d in (2, 1, 3):
            send(
                tb.at[j, d, :, pl.ds(low, width)], here(j, 4 - d, low, width),
                s4.at[i, j], r4.at[i, j], line_peer(q, d, c),
            )
        pltpu.make_async_copy(
            tb.at[j, 0, :, pl.ds(low, width)], here(j, 0, low, width), own_sem.at[i, j]
        ).start()

    settles = [(j, 0, PIECE) for j in PARTS[0]]
    settles += [(j, 0, PIECE // 2) for j in PARTS[1]]
    settles += [(j, PIECE // 2, PIECE // 2) for j in PARTS[1]]
    for j in range(PIECES):
        tsum[j] = summed(j, 0, 0, PIECE)
    for j, low, width in settles:
        settle(j, low, width)

    for q in range(CHUNKS):
        for d in range(LINE):
            if d > 0:
                whole(aux.at[q, d], sa.at[q, d], ra.at[q, d]).wait_send()
                whole(codes.at[q, d], sl.at[q, d], rl.at[q, d]).wait_send()
                whole(xa.at[q, 0, d], s1.at[q, d], r1.at[q, d]).wait_send()
            for e in (1, 3):
                whole(xa.at[q, e, d], sn.at[q, e, d], rn.at[q, e, d]).wait_send()
        whole(xa.at[q, 2], sn.at[q, 2, 0], rn.at[q, 2, 0]).wait_send()
        for h in range(2):
            part = rb.at[q, h] if h else rb.at[q, 0, pl.ds(0, 3)]
            whole(part, s2.at[q, h], r2.at[q, h]).wait_send()
    for j in range(PIECES):
        bulk(ob, j, 0, 0, PIECE, s3, r3).wait_send()
    for j, low, width in settles:
        i = 1 if low else 0
        bulk(ob, j, 1, low, width, s3, r3).wait_send()
        part = tb.at[j, pl.ds(0, 3), :, pl.ds(low, width)]
        whole(part, s4.at[i, j], r4.at[i, j]).wait()
        pltpu.make_async_copy(
            tb.at[j, 0, :, pl.ds(low, width)], here(j, 0, low, width), own_sem.at[i, j]
        ).wait()


def local(
    tokens, norm_gain, expert_ids, expert_scores, group_prob, gate_weight, up_weight, down_weight
):
    hbm = pl.BlockSpec(memory_space=pl.ANY)
    bf16, f32 = jnp.bfloat16, jnp.float32
    dma = pltpu.SemaphoreType.DMA
    width = CHUNKS * CHUNK
    rows = pltpu.VMEM((PIECES, 32, 16, PIECE), bf16)
    line = (CHUNKS, LINE)
    parts = pl.pallas_call(
        step_kernel,
        out_shape=jax.ShapeDtypeStruct((LINE, TOK, width), bf16),
        in_specs=[hbm] * 8,
        out_specs=hbm,
        scratch_shapes=[
            pltpu.VMEM((TOK, width), bf16),
            pltpu.VMEM((1, width), f32),
            pltpu.VMEM((4, TOK), jnp.int32),
            pltpu.VMEM((4, TOK), f32),
            pltpu.VMEM((1, TOK), f32),
            pltpu.VMEM((8, 128), f32),
            pltpu.VMEM((width, 2 * FFE), bf16),
            pltpu.VMEM((FFE, width), bf16),
            pltpu.VMEM(line + (LINE, TOK, CHUNK), bf16),
            pltpu.VMEM(line + (8, 128), f32),
            pltpu.VMEM(line + (8, 128), f32),
            pltpu.VMEM(line + (2, LINE, 16, CHUNK), bf16),
            pltpu.VMEM((CHUNKS, 2, LINE, LINE, 16, CHUNK), bf16),
            pltpu.VMEM((ROWS, width), bf16),
            rows,
            rows,
            pltpu.VMEM((PIECES, LINE * TOK, PIECE), f32),
            pltpu.VMEM((PIECES, LINE, TOK, PIECE), bf16),
            pltpu.VMEM((CHUNKS, 2, 256, ROWS), bf16),
            dma((5,)), dma((3,)), dma((2, PIECES)),
            dma(line), dma(line),
            dma(line), dma(line),
            dma(line), dma(line),
            dma(line + (LINE,)), dma(line + (LINE,)),
            dma((CHUNKS, 2)), dma((CHUNKS, 2)),
            dma((3, PIECES)), dma((3, PIECES)),
            dma((2, PIECES)), dma((2, PIECES)),
        ],
        compiler_params=pltpu.CompilerParams(
            collective_id=0, has_side_effects=True, vmem_limit_bytes=60 * 2**20
        ),
        name="expert_step",
    )(
        tokens, norm_gain[None, :], expert_ids.T, expert_scores.T, group_prob[None, :],
        gate_weight, up_weight, down_weight,
    )
    terms = [parts[s].astype(f32) for s in range(LINE)]
    return ((terms[0] + terms[1]) + (terms[2] + terms[3])).astype(bf16)


def solution(mesh):
    in_specs = (
        P("ep", None),
        P(),
        P("ep", None),
        P("ep", None),
        P("ep"),
        P("ep", None, None),
        P("ep", None, None),
        P("ep", None, None),
    )
    out_specs = P("ep", None)
    return jax.shard_map(local, mesh=mesh, in_specs=in_specs, out_specs=out_specs, check_vma=False)
```

time: 67.5 us -> 65.3 us (0.967)
  Pallas kernels: 65.3 us -> 63.1 us
    pallas_call x1, Pallas kernels: 65.3 us -> 63.1 us  [local(): pl.pallas_call(step_kernel, out_shape=jax.ShapeDtypeStruct((LINE, TOK, wi...]
where the time goes in v3:
time: 65.3 us; the launch traced here: 65.1 us
  Pallas kernels  63.1 us (97%)
  other arithmetic  2 us (3%)
    pallas_call x1, Pallas kernels, local(): pl.pallas_call(step_kernel, out_shape=jax.ShapeDtypeStruct((LINE, TOK, wi...  63.1 us
    convert_element_type x1, other arithmetic, local(): return (terms[0] + terms[1] + (terms[2] + terms[3])).astype(bf16)  2 us

profile of v3, /device:TPU:1, one launch (start us, length us, event | category | flops | bytes accessed | tf_op | source)
XLA Modules:
  0.0 65.1 jit_solution(8611231418692175479)
XLA Ops:
  0.0 63.1 %expert_step.1 = bf16[4,32,3072]{2,1,0:T(8,128)(2,1)} custom-call(bf16[32,3072]{1,0:T(8,128)(2,1)} %tok_hbm.1, f32[1,3072]{1,0:T(1,128)} %bitcast.6, s32[4,32]{1,0:T(4,128)} %bitcast.7, f32[4,32]{1,0:T(4,128)} %bitcast.8, f32[1,32]{1,0:T(1,128)} %bitcast.9, bf16[1,3072,384]{2,1,0:T(8,128)(2,1)} %gate_hbm.1, bf16[1,3072,384]{2,1,0:T(8,128)(2,1)} %up_hbm.1, ...), custom_call_target="tpu_custom_call" | custom-call | tf_op jit(solution)/shard_map/expert_step/pallas_call | solution.py:412
  63.1 2.0 %fusion = bf16[32,3072]{1,0:T(8,128)(2,1)} fusion(bf16[4,32,3072]{2,1,0:T(8,128)(2,1)} %expert_step.1), kind=kLoop, calls=%fused_computation.1 | loop fusion | flops 786432 | bytes 983040 | tf_op jit(solution)/shard_map/convert_element_type | solution.py:455

commit v4 on v3

--- a/solution.py
+++ b/solution.py
@@ -12,9 +12,9 @@
 TOK = 32
 CHUNK = 1024
 CHUNKS = 3
-PIECE = 512
-PIECES = 6
-PARTS = ((0, 1, 2), (3, 4, 5))
+PIECE = 256
+PIECES = 12
+PARTS = ((0, 1, 2), (3, 4, 5), (6, 7, 8), (9, 10, 11))
 ROWS = 256
 FFE = 384
 STRIDE = (7, 11, 13)
@@ -94,7 +94,7 @@
                 )
     pl.semaphore_signal(barrier, inc=1, device_id=(device(z, y, x, other),), device_id_type=MESH)
 
-    for copy in smalls[:2]:
+    for copy in smalls:
         copy.wait()
 
     values = tok_ref[...].astype(jnp.float32)
@@ -117,8 +117,6 @@
                 line_peer((q + 1) % 3, step, c),
             )
 
-    for copy in smalls[2:]:
-        copy.wait()
     ids = ids_ref[...]
     scores = score_ref[...]
     exp_scores = jnp.exp(scores - jnp.max(scores, axis=0, keepdims=True))
@@ -166,10 +164,8 @@
             device_id=(me,), device_id_type=MESH,
         )
 
-    def bulk(ref, j, h, low, width, send_sem, recv_sem):
-        part = ref.at[j, pl.ds(0, 15 + h), :, pl.ds(low, width)]
-        i = (1 + h) if low else h
-        return whole(part, send_sem.at[i, j], recv_sem.at[i, j])
+    def bulk(ref, j, h, send_sem, recv_sem):
+        return whole(ref.at[j, pl.ds(0, 15 + h)], send_sem.at[h, j], recv_sem.at[h, j])
 
     def row_code(q, h, shape, dim):
         r = iota(shape, dim)
@@ -177,23 +173,23 @@
         core = c if h == 0 else other
         return (plane_peer(q, a, b, core) * 16 + low).astype(jnp.float32)
 
-    def exchange(h, part, low=0, width=PIECE):
+    def exchange(h, part):
         core = c if h == 0 else other
+        last = h == 1 and part is PARTS[-1]
 
         def body(t, carry):
             for j in part:
                 q = j % 3
-                turn = t if low else (t * STRIDE[q]) % 16
+                turn = t if last else (t * STRIDE[q]) % 16
                 a, b = rel(plane[q][0], turn // 4), rel(plane[q][1], turn % 4)
-                i = (1 + h) if low else h
                 send(
-                    ob.at[j, h * 16 + a * 4 + b, :, pl.ds(low, width)],
-                    gb.at[j, h * 16 + plane[q][0] * 4 + plane[q][1], :, pl.ds(low, width)],
-                    s3.at[i, j], r3.at[i, j], plane_peer(q, a, b, core),
+                    ob.at[j, h * 16 + a * 4 + b],
+                    gb.at[j, h * 16 + plane[q][0] * 4 + plane[q][1]],
+                    s3.at[h, j], r3.at[h, j], plane_peer(q, a, b, core),
                 )
             return carry
 
-        if low:
+        if last:
             for t in FAR:
                 body(t, 0)
         else:
@@ -255,9 +251,18 @@
                         s2.at[q, h], r2.at[q, h], line_peer((q + 2) % 3, step, core),
                     )
 
+    for d in (0,):
+        for q in range(CHUNKS):
+            for step, low in ((3, 0), (1, half)):
+                e = 4 - step
+                whole(xa.at[q, e, d], sn.at[q, e, d], rn.at[q, e, d]).wait_recv()
+                send(
+                    xa.at[q, e, d, :, pl.ds(low, half)], xa.at[q, 2, d, :, pl.ds(low, half)],
+                    sn.at[q, 2, 0], rn.at[q, 2, 0], line_peer((q + 1) % 3, step, c),
+                )
     select(0)
     deliver(0, 0)
-    for d in (0, 1, 3, 2):
+    for d in (1, 3, 2):
         for q in range(CHUNKS):
             for step, low in ((3, 0), (1, half)):
                 e = 4 - step
@@ -339,42 +344,34 @@
                     hidden[j % 3], w_out[:, columns(j)], preferred_element_type=jnp.float32
                 )
                 ob[j, h * 16:(h + 1) * 16] = made.astype(jnp.bfloat16).reshape(16, 16, PIECE)
-            if h == 1 and part is PARTS[1]:
-                exchange(1, part, 0, PIECE // 2)
-                exchange(1, part, PIECE // 2, PIECE // 2)
-            else:
-                exchange(h, part)
-
-    def here(j, slot, low, width):
-        return parts_ref.at[slot, :, pl.ds(columns(j).start + low, width)]
-
-    def summed(j, h, low, width):
-        bulk(gb, j, h, low, width, s3, r3).wait_recv()
-        rows = gb[j, h * 16:(h + 1) * 16, :, low:low + width].reshape(ROWS, width)
+            exchange(h, part)
+
+    def here(j, slot):
+        return parts_ref.at[slot, :, pl.ds(columns(j).start, PIECE)]
+
+    def summed(j, h):
+        rows = gb[j, h * 16:(h + 1) * 16].reshape(ROWS, PIECE)
         both = jnp.dot(wm[j % 3, h], rows, preferred_element_type=jnp.float32)
         return both[0:128] + both[128:256]
 
-    def settle(j, low, width):
-        q = j % 3
-        total = tsum[j, :, low:low + width] + summed(j, 1, low, width)
-        tb[j, :, :, low:low + width] = total.astype(jnp.bfloat16).reshape(LINE, TOK, width)
-        i = 1 if low else 0
+    for part in PARTS:
+        for j in part:
+            bulk(gb, j, 0, s3, r3).wait_recv()
+        for j in part:
+            tsum[j] = summed(j, 0)
+    for part in PARTS:
+        for j in part:
+            bulk(gb, j, 1, s3, r3).wait_recv()
+        for j in part:
+            total = tsum[j] + summed(j, 1)
+            tb[j] = total.astype(jnp.bfloat16).reshape(LINE, TOK, PIECE)
         for d in (2, 1, 3):
-            send(
-                tb.at[j, d, :, pl.ds(low, width)], here(j, 4 - d, low, width),
-                s4.at[i, j], r4.at[i, j], line_peer(q, d, c),
-            )
-        pltpu.make_async_copy(
-            tb.at[j, 0, :, pl.ds(low, width)], here(j, 0, low, width), own_sem.at[i, j]
-        ).start()
-
-    settles = [(j, 0, PIECE) for j in PARTS[0]]
-    settles += [(j, 0, PIECE // 2) for j in PARTS[1]]
-    settles += [(j, PIECE // 2, PIECE // 2) for j in PARTS[1]]
-    for j in range(PIECES):
-        tsum[j] = summed(j, 0, 0, PIECE)
-    for j, low, width in settles:
-        settle(j, low, width)
+            for j in part:
+                send(
+                    tb.at[j, d], here(j, 4 - d), s4.at[j], r4.at[j], line_peer(j % 3, d, c)
+                )
+        for j in part:
+            pltpu.make_async_copy(tb.at[j, 0], here(j, 0), own_sem.at[j]).start()
 
     for q in range(CHUNKS):
         for d in range(LINE):
@@ -389,15 +386,10 @@
             part = rb.at[q, h] if h else rb.at[q, 0, pl.ds(0, 3)]
             whole(part, s2.at[q, h], r2.at[q, h]).wait_send()
     for j in range(PIECES):
-        bulk(ob, j, 0, 0, PIECE, s3, r3).wait_send()
-    for j, low, width in settles:
-        i = 1 if low else 0
-        bulk(ob, j, 1, low, width, s3, r3).wait_send()
-        part = tb.at[j, pl.ds(0, 3), :, pl.ds(low, width)]
-        whole(part, s4.at[i, j], r4.at[i, j]).wait()
-        pltpu.make_async_copy(
-            tb.at[j, 0, :, pl.ds(low, width)], here(j, 0, low, width), own_sem.at[i, j]
-        ).wait()
+        for h in range(2):
+            bulk(ob, j, h, s3, r3).wait_send()
+        whole(tb.at[j, pl.ds(0, 3)], s4.at[j], r4.at[j]).wait()
+        pltpu.make_async_copy(tb.at[j, 0], here(j, 0), own_sem.at[j]).wait()
 
 
 def local(
@@ -434,14 +426,14 @@
             pltpu.VMEM((PIECES, LINE * TOK, PIECE), f32),
             pltpu.VMEM((PIECES, LINE, TOK, PIECE), bf16),
             pltpu.VMEM((CHUNKS, 2, 256, ROWS), bf16),
-            dma((5,)), dma((3,)), dma((2, PIECES)),
+            dma((5,)), dma((3,)), dma((PIECES,)),
             dma(line), dma(line),
             dma(line), dma(line),
             dma(line), dma(line),
             dma(line + (LINE,)), dma(line + (LINE,)),
             dma((CHUNKS, 2)), dma((CHUNKS, 2)),
-            dma((3, PIECES)), dma((3, PIECES)),
             dma((2, PIECES)), dma((2, PIECES)),
+            dma((PIECES,)), dma((PIECES,)),
         ],
         compiler_params=pltpu.CompilerParams(
             collective_id=0, has_side_effects=True, vmem_limit_bytes=60 * 2**20

time: 65.3 us -> 64.9 us (level)
  no operation moved by 1% of the time
where the time goes in v4:
time: 64.9 us; the launch traced here: 64.7 us
  Pallas kernels  62.7 us (97%)
  other arithmetic  2 us (3%)
    pallas_call x1, Pallas kernels, local(): pl.pallas_call(step_kernel, out_shape=jax.ShapeDtypeStruct((LINE, TOK, wi...  62.7 us
    convert_element_type x1, other arithmetic, local(): return (terms[0] + terms[1] + (terms[2] + terms[3])).astype(bf16)  2 us

profile of v4, /device:TPU:1, one launch (start us, length us, event | category | flops | bytes accessed | tf_op | source)
XLA Modules:
  0.0 64.7 jit_solution(3554250586467078292)
XLA Ops:
  0.0 62.7 %expert_step.1 = bf16[4,32,3072]{2,1,0:T(8,128)(2,1)} custom-call(bf16[32,3072]{1,0:T(8,128)(2,1)} %tok_hbm.1, f32[1,3072]{1,0:T(1,128)} %bitcast.6, s32[4,32]{1,0:T(4,128)} %bitcast.7, f32[4,32]{1,0:T(4,128)} %bitcast.8, f32[1,32]{1,0:T(1,128)} %bitcast.9, bf16[1,3072,384]{2,1,0:T(8,128)(2,1)} %gate_hbm.1, bf16[1,3072,384]{2,1,0:T(8,128)(2,1)} %up_hbm.1, ...), custom_call_target="tpu_custom_call" | custom-call | tf_op jit(solution)/shard_map/expert_step/pallas_call | solution.py:404
  62.7 2.0 %fusion = bf16[32,3072]{1,0:T(8,128)(2,1)} fusion(bf16[4,32,3072]{2,1,0:T(8,128)(2,1)} %expert_step.1), kind=kLoop, calls=%fused_computation.1 | loop fusion | flops 786432 | bytes 983040 | tf_op jit(solution)/shard_map/convert_element_type | solution.py:447

commit v5 on v4

--- a/solution.py
+++ b/solution.py
@@ -68,6 +68,15 @@
             device(a, y, b, core),
             device(z, b, a, core),
         )[q]
+
+    barrier = pltpu.get_barrier_semaphore()
+    for step in (2, 1, 3):
+        for q in range(CHUNKS):
+            for core in (c, other):
+                pl.semaphore_signal(
+                    barrier, inc=1, device_id=(line_peer(q, step, core),), device_id_type=MESH
+                )
+    pl.semaphore_signal(barrier, inc=1, device_id=(device(z, y, x, other),), device_id_type=MESH)
 
     smalls = [
         pltpu.make_async_copy(src, dst, in_sem.at[i])
@@ -85,15 +94,6 @@
     ]
     for copy in weights:
         copy.start()
-    barrier = pltpu.get_barrier_semaphore()
-    for step in (2, 1, 3):
-        for q in range(CHUNKS):
-            for core in (c, other):
-                pl.semaphore_signal(
-                    barrier, inc=1, device_id=(line_peer(q, step, core),), device_id_type=MESH
-                )
-    pl.semaphore_signal(barrier, inc=1, device_id=(device(z, y, x, other),), device_id_type=MESH)
-
     for copy in smalls:
         copy.wait()
 
@@ -169,7 +169,8 @@
 
     def row_code(q, h, shape, dim):
         r = iota(shape, dim)
-        a, b, low = r >> 6, (r >> 4) & 3, r & 15
+        low = r & 15
+        a, b = (plane[q][0] + (r >> 6)) & 3, (plane[q][1] + (r >> 4)) & 3
         core = c if h == 0 else other
         return (plane_peer(q, a, b, core) * 16 + low).astype(jnp.float32)
 
@@ -181,11 +182,12 @@
             for j in part:
                 q = j % 3
                 turn = t if last else (t * STRIDE[q]) % 16
-                a, b = rel(plane[q][0], turn // 4), rel(plane[q][1], turn % 4)
+                a, b = turn // 4, turn % 4
                 send(
-                    ob.at[j, h * 16 + a * 4 + b],
-                    gb.at[j, h * 16 + plane[q][0] * 4 + plane[q][1]],
-                    s3.at[h, j], r3.at[h, j], plane_peer(q, a, b, core),
+                    ob.at[j, h * 16 + turn],
+                    gb.at[j, h * 16 + ((4 - a) % 4) * 4 + (4 - b) % 4],
+                    s3.at[h, j], r3.at[h, j],
+                    plane_peer(q, rel(plane[q][0], a), rel(plane[q][1], b), core),
                 )
             return carry
 
@@ -196,8 +198,7 @@
             lax.fori_loop(1 - h, 16, body, 0)
         if h == 0:
             for j in part:
-                mine = plane[j % 3][0] * 4 + plane[j % 3][1]
-                gb[j, pl.ds(mine, 1)] = ob[j, pl.ds(mine, 1)]
+                gb[j, 0] = ob[j, 0]
 
     for q in range(CHUNKS):
         for d in (1, 3, 2):
@@ -307,18 +308,15 @@
 
     def leaving(q, o):
         zz, yy, xx, slot = o >> 6, (o >> 4) & 3, (o >> 2) & 3, o & 3
-        az, ay, ax = (zz + z) & 3, (yy + y) & 3, (xx + x) & 3
-        if q == 0:
-            return az * 64 + ay * 16 + xx * 4 + slot
         if q == 1:
-            return az * 64 + ax * 16 + yy * 4 + slot
-        return ax * 64 + ay * 16 + zz * 4 + slot
+            return zz * 64 + xx * 16 + yy * 4 + slot
+        return xx * 64 + yy * 16 + zz * 4 + slot
 
     gather_order = [None] + [
         one_hot(arrived(q, iota(square, 0)) == iota(square, 1)) for q in (1, 2)
     ]
-    spread_order = [
-        one_hot(leaving(q, iota(square, 1)) == iota(square, 0)) for q in range(CHUNKS)
+    spread_order = [None] + [
+        one_hot(leaving(q, iota(square, 1)) == iota(square, 0)) for q in (1, 2)
     ]
 
     def ordered(order, rows):
@@ -332,6 +330,7 @@
         for q in range(CHUNKS):
             part = rb.at[q, h] if h else rb.at[q, 0, pl.ds(0, 3)]
             whole(part, s2.at[q, h], r2.at[q, h]).wait_recv()
+        for q in range(CHUNKS):
             rows = rb[q, h].reshape(ROWS, CHUNK)
             xp[:, q * CHUNK:(q + 1) * CHUNK] = ordered(gather_order[q], rows)
         acts = jnp.dot(xp[...], w_in[...], preferred_element_type=jnp.float32)

time: 64.9 us -> 64.9 us (level)
  no operation moved by 1% of the time
where the time goes in v5:
time: 64.9 us; the launch traced here: 64.7 us
  Pallas kernels  62.7 us (97%)
  other arithmetic  2 us (3%)
    pallas_call x1, Pallas kernels, local(): pl.pallas_call(step_kernel, out_shape=jax.ShapeDtypeStruct((LINE, TOK, wi...  62.7 us
    convert_element_type x1, other arithmetic, local(): return (terms[0] + terms[1] + (terms[2] + terms[3])).astype(bf16)  2 us

profile of v5, /device:TPU:1, one launch (start us, length us, event | category | flops | bytes accessed | tf_op | source)
XLA Modules:
  0.0 64.7 jit_solution(5850879805055628720)
XLA Ops:
  0.0 62.7 %expert_step.1 = bf16[4,32,3072]{2,1,0:T(8,128)(2,1)} custom-call(bf16[32,3072]{1,0:T(8,128)(2,1)} %tok_hbm.1, f32[1,3072]{1,0:T(1,128)} %bitcast.6, s32[4,32]{1,0:T(4,128)} %bitcast.7, f32[4,32]{1,0:T(4,128)} %bitcast.8, f32[1,32]{1,0:T(1,128)} %bitcast.9, bf16[1,3072,384]{2,1,0:T(8,128)(2,1)} %gate_hbm.1, bf16[1,3072,384]{2,1,0:T(8,128)(2,1)} %up_hbm.1, ...), custom_call_target="tpu_custom_call" | custom-call | tf_op jit(solution)/shard_map/expert_step/pallas_call | solution.py:403
  62.7 2.0 %fusion = bf16[32,3072]{1,0:T(8,128)(2,1)} fusion(bf16[4,32,3072]{2,1,0:T(8,128)(2,1)} %expert_step.1), kind=kLoop, calls=%fused_computation.1 | loop fusion | flops 786432 | bytes 983040 | tf_op jit(solution)/shard_map/convert_element_type | solution.py:446
